TPU v7x, 32 devices: a whole 2x2x4 slice. The times are simulated.
32 devices in a mesh: fs: 16 (over z, y, core), tp: 2 (over x).
Axes of the slice: x: 2, y: 2, z: 4, core: 2. Of those that a mesh axis runs over, the one named last changes fastest.
Arguments:
- tokens: bfloat16 [8192, 2048], P('fs', 'tp'), may hold values from -6 to 6
- norm_gain: float32 [2048], P('fs'), may hold values from 0.1 to 1.9
- up_trained: float32 [2048, 4096], P('fs', 'tp'), may hold values from -0.125 to 0.125
- down_trained: float32 [4096, 2048], P('fs', 'tp'), may hold values from -0.09375 to 0.09375
Outputs:
- up_serving: bfloat16 [2048, 4096], P(None, 'tp')
- down_serving: bfloat16 [4096, 2048], P('tp')
- mixed: bfloat16 [8192, 2048], P('fs', 'tp')
All inputs are finite; a program needn't handle non-finite values.
Results may differ from a plain program's by a relative error of at most 0.013.
Values may be sent and summed in bfloat16 or wider, within the bound.
A program may use at most 128 MiB of HBM per device.

v0:
```python
import jax
import jax.numpy as jnp
from jax import lax
from jax.sharding import PartitionSpec as P


def per_device(tokens, norm_gain, up_trained, down_trained):
    up_piece = (norm_gain[:, None] * up_trained).astype(jnp.bfloat16)
    up_serving = lax.all_gather(up_piece, "fs", axis=0, tiled=True)
    down_piece = down_trained.astype(jnp.bfloat16)
    group_count = lax.axis_size("fs")
    pair_count = lax.axis_size("tp")
    sliver = down_piece.shape[1] // group_count
    flipped = down_piece.T
    narrow = lax.all_to_all(flipped, "fs", split_axis=0, concat_axis=1, tiled=True)
    regrouped = lax.all_to_all(narrow, "tp", split_axis=1, concat_axis=0, tiled=True)
    spread = lax.all_gather(regrouped, "fs", axis=0, tiled=True)
    block_width = spread.shape[1]
    ordered = spread.reshape(group_count, pair_count, sliver, block_width).transpose(1, 0, 2, 3)
    down_serving = ordered.reshape(pair_count * group_count * sliver, block_width).T
    features = lax.all_gather(tokens, "tp", axis=1, tiled=True)
    widened = features.astype(jnp.float32)
    scale = lax.rsqrt(jnp.mean(widened * widened, axis=-1, keepdims=True) + 1e-06)
    normed = (widened * scale).astype(jnp.bfloat16)
    preact = jnp.dot(normed, up_serving, preferred_element_type=jnp.float32)
    hidden = jnp.square(jnp.maximum(preact, 0.0)).astype(jnp.bfloat16)
    partial_out = jnp.dot(hidden, down_serving, preferred_element_type=jnp.float32)
    summed = lax.psum_scatter(
        partial_out.astype(jnp.bfloat16), "tp", scatter_dimension=1, tiled=True
    )
    return (up_serving, down_serving, summed)


def solution(mesh):
    placed = (P("fs", "tp"), P("fs"), P("fs", "tp"), P("fs", "tp"))
    return jax.shard_map(
        per_device,
        mesh=mesh,
        in_specs=placed,
        out_specs=(P(None, "tp"), P("tp", None), P("fs", "tp")),
        check_vma=False,
    )
```

profile of v0, /device:TPU:0, one launch (start us, length us, event | category | flops | bytes accessed | tf_op | source)
XLA Modules:
  0.0 264.8 jit_solution(10153047460143289739)
XLA Ops:
  7.2 0.0 copy-start.2
  7.2 0.0 copy-start.1
  7.2 0.0 all-gather.8.cloned.1.call-start
  7.2 0.7 all-gather.8.cloned.1.call-update
  7.9 0.0 all-gather.6.cloned.1.call-start
  8.0 1.4 copy.12
  9.4 21.5 %all_to_all.35 = bf16[16,64,256]{2,1,0:T(8,128)(2,1)S(1)} all-to-all(bf16[16,64,256]{2,1,0:T(8,128)(2,1)S(1)} %bitcast.23), channel_id=1, replica_groups=mesh['fs'=16,'tp'=2] {'fs'}, dimensions={0} | all-to-all | bytes 1048576 | tf_op jit(solution)/shard_map/all_to_all | solution.py:15
  30.9 0.3 copy.13
  31.2 0.1 all_to_all.29
  31.3 0.2 copy.14
  31.5 17.9 %all_to_all.36 = bf16[64,2,2048]{2,0,1:T(8,128)(2,1)} all-to-all(bf16[64,2,2048]{2,0,1:T(8,128)(2,1)S(1)} %copy.14), channel_id=1, replica_groups=mesh['fs'=16,'tp'=2] {'tp'}, dimensions={1} | all-to-all | bytes 1048576 | tf_op jit(solution)/shard_map/all_to_all | solution.py:16
  49.4 0.0 all-gather.6.cloned.1.call-update
  49.4 0.0 all-gather.4.cloned.1.call-start
  49.4 0.0 copy-done.2
  49.4 0.0 copy-done.1
  49.5 0.9 multiply_convert_fusion.1
  50.4 0.0 all-gather.4.cloned.1.call-update
  50.4 0.0 reduce-scatter.2.cloned.1.call-start
  50.5 0.6 all-gather.8.cloned.1.call-done
  51.0 2.1 fusion
  53.1 74.4 %all-gather.6.cloned.1.call-done = bf16[2048,2048]{1,0:T(8,128)(2,1)} async-done(((bf16[128,2048]{1,0:T(8,128)(2,1)}), bf16[2048,2048]{1,0:T(8,128)(2,1)}) %all-gather.6.cloned.1.call-update) | async-done | bytes 8388624 | tf_op jit(solution)/shard_map/all_gather | solution.py:17
  127.5 0.0 copy-start
  127.5 8.6 %copy.15 = bf16[2,16,64,2048]{3,2,1,0:T(8,128)(2,1)} copy(bf16[2,16,64,2048]{3,2,0,1:T(8,128)(2,1)} %bitcast.22) | data formatting | bytes 16777216 | tf_op jit(solution)/shard_map/transpose | solution.py:19
  136.1 67.1 %all-gather.4.cloned.1.call-done = bf16[2048,2048]{1,0:T(8,128)(2,1)} async-done(((bf16[128,2048]{1,0:T(8,128)(2,1)}), bf16[2048,2048]{1,0:T(8,128)(2,1)}) %all-gather.4.cloned.1.call-update) | async-done | bytes 8388624 | tf_op jit(solution)/shard_map/all_gather | solution.py:9
  203.1 0.0 copy-done
  203.2 16.0 %convolution_convert_fusion = bf16[512,2048]{1,0:T(8,128)(2,1)} fusion(bf16[2048,2048]{1,0:T(8,128)(2,1)} %bitcast.20, bf16[2048,2048]{1,0:T(8,128)(2,1)} %all-gather.4.cloned.1.call-done, bf16[512,2048]{1,0:T(8,128)(2,1)S(1)} %copy-done, f32[512]{0:T(512)S(1)} %add_rsqrt_fusion), kind=kOutput, calls=%fused_computation.5 | convolution fusion | flops 8597274624 | bytes 20973568 | tf_op jit(solution)/shard_map/dot_general | solution.py:27
  219.1 0.0 reduce-scatter.2.cloned.1.call-update
  219.2 11.9 %copy.16 = bf16[2048,2048]{1,0:T(8,128)(2,1)} copy(bf16[2048,2048]{0,1:T(8,128)(2,1)} %bitcast.21) | data formatting | bytes 16777216
  231.1 18.7 %reduce-scatter.2.cloned.1.call-done = bf16[512,1024]{1,0:T(8,128)(2,1)} async-done(((bf16[512,2048]{1,0:T(8,128)(2,1)}), bf16[512,1024]{1,0:T(8,128)(2,1)}) %reduce-scatter.2.cloned.1.call-update) | async-done | bytes 1048592 | tf_op jit(solution)/shard_map/reduce_scatter | solution.py:28
  249.8 8.4 %copy.18 = bf16[2048,2048]{1,0:T(8,128)(2,1)} copy(bf16[2048,2048]{1,0:T(8,128)(2,1)} %all-gather.4.cloned.1.call-done) | data formatting | bytes 16777216
  (1 shorter events, 0.0 us)
Async XLA Ops:
  7.2 42.3 %copy-start.2 = (f32[128]{0:T(128)S(1)}, f32[128]{0:T(128)}, u32[]{:S(2)}) copy-start(f32[128]{0:T(128)} %param.5) | copy-start | bytes 1540
  7.2 42.3 %copy-start.1 = (f32[128,2048]{1,0:T(8,128)S(1)}, f32[128,2048]{1,0:T(8,128)}, u32[]{:S(2)}) copy-start(f32[128,2048]{1,0:T(8,128)} %param.6) | copy-start | bytes 3145732
  7.2 43.8 %all-gather.8.cloned.1.call-start = ((), (), s32[]{:S(2)}) async-start(), calls=%async_computation.5 | async-start | bytes 3145728 | tf_op jit(solution)/shard_map/all_gather | solution.py:21
  7.9 119.6 %all-gather.6.cloned.1.call-start = ((), (), s32[]{:S(2)}) async-start(), calls=%async_computation.4 | async-start | bytes 8912896 | tf_op jit(solution)/shard_map/all_gather | solution.py:17
  49.4 153.8 %all-gather.4.cloned.1.call-start = ((), (), s32[]{:S(2)}) async-start(), calls=%async_computation.3 | async-start | bytes 8912896 | tf_op jit(solution)/shard_map/all_gather | solution.py:9
  50.4 199.4 %reduce-scatter.2.cloned.1.call-start = ((), (), s32[]{:S(2)}) async-start(), calls=%async_computation.6 | async-start | bytes 3145728 | tf_op jit(solution)/shard_map/reduce_scatter | solution.py:28
  127.5 75.7 %copy-start = (bf16[512,2048]{1,0:T(8,128)(2,1)S(1)}, bf16[512,2048]{1,0:T(8,128)(2,1)}, u32[]{:S(2)}) copy-start(bf16[512,2048]{1,0:T(8,128)(2,1)} %all-gather.8.cloned.1.call-done) | copy-start | bytes 6291460
Sparse Core Ops, SparseCore 0:
  9.5 41.4 all-gather.7
  53.2 74.2 all-gather.5
  130.2 72.8 all-gather.3
  219.3 30.4 reduce-scatter.1
where the time goes:
time: 265 us
  waiting for transfers between devices  161 us (61%)
  blocking collectives  39.4 us (15%)
  local copies, waits for them, and re-layouts  31 us (12%)
  matrix products  16 us (6%)
  between operations  13.8 us (5%)
  other arithmetic  3 us (1%)
    all_gather x1, waiting for transfers between devices, per_device(): spread = lax.all_gather(regrouped, 'fs', axis=0, tiled=True)  74.4 us
    all_gather x1, waiting for transfers between devices, per_device(): up_serving = lax.all_gather(up_piece, 'fs', axis=0, tiled=True)  67.1 us
    unnamed x9, local copies, waits for them, and re-layouts  21.8 us
    all_to_all x1, blocking collectives, per_device(): lax.all_to_all(flipped, 'fs', split_axis=0, concat_axis=1, tiled=True)  21.5 us
    reduce_scatter x1, waiting for transfers between devices, per_device(): lax.psum_scatter(partial_out.astype(jnp.bfloat16), 'tp', scatter_dimensio...  18.7 us
    all_to_all x1, blocking collectives, per_device(): lax.all_to_all(narrow, 'tp', split_axis=1, concat_axis=0, tiled=True)  17.9 us
    dot_general x1, matrix products, per_device(): jnp.dot(hidden, down_serving, preferred_element_type=jnp.float32)  16 us
    transpose x1, local copies, waits for them, and re-layouts, per_device(): spread.reshape(group_count, pair_count, sliver, block_width)  8.59 us
  transfers between devices with their start and end apart: 4, of which 4 were waited for; matrix products, arithmetic and copies ran while one was open for 10% of the time, Pallas kernels for 0%

commit v1 on v0

--- a/solution.py
+++ b/solution.py
@@ -2,6 +2,7 @@
 import jax.numpy as jnp
 from jax import lax
 from jax.sharding import PartitionSpec as P
+from jax.lax import all_to_all, axis_size
 
 
 def per_device(tokens, norm_gain, up_trained, down_trained):
@@ -14,7 +15,8 @@
     flipped = down_piece.T
     narrow = lax.all_to_all(flipped, "fs", split_axis=0, concat_axis=1, tiled=True)
     regrouped = lax.all_to_all(narrow, "tp", split_axis=1, concat_axis=0, tiled=True)
-    spread = lax.all_gather(regrouped, "fs", axis=0, tiled=True)
+    kept_arr = all_to_all(jnp.stack([regrouped for _ in range(axis_size("fs"))]), "fs", 0, 0)
+    spread = jnp.concatenate(kept_arr, 0)
     block_width = spread.shape[1]
     ordered = spread.reshape(group_count, pair_count, sliver, block_width).transpose(1, 0, 2, 3)
     down_serving = ordered.reshape(pair_count * group_count * sliver, block_width).T

time: 265 us -> 362 us (1.37)
  waiting for transfers between devices: 161 us -> 249 us
  starting transfers between devices: 0.16 us -> 5.04 us
  local copies, waits for them, and re-layouts: 31 us -> 35.7 us
    all_to_all x0 -> x1, waiting for transfers between devices: none -> 198 us  [per_device(): all_to_all(jnp.stack([regrouped for _ in range(axis_size('fs'))]), 'fs',...]
    all_gather x1 -> x0, waiting for transfers between devices: 74.4 us -> none  [per_device(): spread = lax.all_gather(regrouped, 'fs', axis=0, tiled=True)]
    all_gather x1, waiting for transfers between devices: 67.1 us -> 0.01 us  [per_device(): up_serving = lax.all_gather(up_piece, 'fs', axis=0, tiled=True)]
    reduce_scatter x1, waiting for transfers between devices: 18.7 us -> 50.7 us  [per_device(): lax.psum_scatter(partial_out.astype(jnp.bfloat16), 'tp', scatter_dimensio...]
    all_to_all x0 -> x1, starting transfers between devices: none -> 4.91 us  [per_device(): all_to_all(jnp.stack([regrouped for _ in range(axis_size('fs'))]), 'fs',...]
    another operation x0 -> x1, local copies, waits for them, and re-layouts: none -> 4.47 us  [per_device(): jnp.stack([regrouped for _ in range(axis_size('fs'))])]
  transfers between devices with their start and end apart: 4 -> 4, of which waited for: 4 -> 2; matrix products, arithmetic and copies ran while one was open for 10% -> 8% of each run, Pallas kernels for 0% -> 0%
where the time goes in v1:
time: 362 us
  waiting for transfers between devices  249 us (69%)
  blocking collectives  38.8 us (11%)
  local copies, waits for them, and re-layouts  35.7 us (10%)
  matrix products  16 us (4%)
  between operations  13.8 us (4%)
  starting transfers between devices  5.04 us (1%)
    all_to_all x1, waiting for transfers between devices, per_device(): all_to_all(jnp.stack([regrouped for _ in range(axis_size('fs'))]), 'fs',...  198 us
    reduce_scatter x1, waiting for transfers between devices, per_device(): lax.psum_scatter(partial_out.astype(jnp.bfloat16), 'tp', scatter_dimensio...  50.7 us
    unnamed x9, local copies, waits for them, and re-layouts  22.1 us
    all_to_all x1, blocking collectives, per_device(): lax.all_to_all(flipped, 'fs', split_axis=0, concat_axis=1, tiled=True)  21.5 us
    all_to_all x1, blocking collectives, per_device(): lax.all_to_all(narrow, 'tp', split_axis=1, concat_axis=0, tiled=True)  17.3 us
    dot_general x1, matrix products, per_device(): jnp.dot(hidden, down_serving, preferred_element_type=jnp.float32)  16 us
    transpose x1, local copies, waits for them, and re-layouts, per_device(): spread.reshape(group_count, pair_count, sliver, block_width)  8.59 us
  transfers between devices with their start and end apart: 4, of which 2 were waited for; matrix products, arithmetic and copies ran while one was open for 8% of the time, Pallas kernels for 0%

profile of v1, /device:TPU:0, one launch (start us, length us, event | category | flops | bytes accessed | tf_op | source)
XLA Modules:
  0.0 361.6 jit_solution(6687419041700266155)
XLA Ops:
  7.2 0.0 all-gather.5.cloned.1.call-start
  7.2 0.7 all-gather.5.cloned.1.call-update
  7.9 1.4 copy.12
  9.3 21.5 %all_to_all.37 = bf16[16,64,256]{2,1,0:T(8,128)(2,1)S(1)} all-to-all(bf16[16,64,256]{2,1,0:T(8,128)(2,1)S(1)} %bitcast.23), channel_id=1, replica_groups=mesh['fs'=16,'tp'=2] {'fs'}, dimensions={0} | all-to-all | bytes 1048576 | tf_op jit(solution)/shard_map/all_to_all | solution.py:16
  30.8 0.3 copy.13
  31.1 0.1 all_to_all.30
  31.2 0.2 copy.14
  31.4 17.3 %all_to_all.38 = bf16[64,2,2048]{2,0,1:T(8,128)(2,1)S(1)} all-to-all(bf16[64,2,2048]{2,0,1:T(8,128)(2,1)S(1)} %copy.14), channel_id=1, replica_groups=mesh['fs'=16,'tp'=2] {'tp'}, dimensions={1} | all-to-all | bytes 1048576 | tf_op jit(solution)/shard_map/all_to_all | solution.py:17
  48.7 4.5 %stack.5 = bf16[16,128,2048]{2,1,0:T(8,128)(2,1)} broadcast(bf16[128,2048]{1,0:T(8,128)(2,1)S(1)} %bitcast.22), dimensions={1,2} | broadcast | bytes 8912896 | tf_op jit(solution)/shard_map/stack | solution.py:18
  53.1 0.0 copy-start.1
  53.2 0.0 copy-start.2
  53.2 4.9 %all-to-all-start.2 = ((bf16[16,128,2048]{2,1,0:T(8,128)(2,1)}), bf16[16,128,2048]{2,1,0:T(8,128)(2,1)}, u32[]{:S(2)}, u32[]{:S(2)}) async-start(bf16[16,128,2048]{2,1,0:T(8,128)(2,1)} %stack.5), calls=%async_computation.2 | async-start | bytes 16777216 | tf_op jit(solution)/shard_map/all_to_all | solution.py:18
  58.1 0.0 all-gather.3.cloned.1.call-start
  58.1 0.0 copy-done.1
  58.1 0.0 copy-done.2
  58.1 0.9 multiply_convert_fusion.1
  59.1 0.0 all-gather.3.cloned.1.call-update
  59.1 0.0 reduce-scatter.2.cloned.1.call-start
  59.1 0.0 all-gather.5.cloned.1.call-done
  59.2 2.1 fusion
  61.2 197.9 %all-to-all-done.2 = bf16[16,128,2048]{2,1,0:T(8,128)(2,1)} async-done(((bf16[16,128,2048]{2,1,0:T(8,128)(2,1)}), bf16[16,128,2048]{2,1,0:T(8,128)(2,1)}, u32[]{:S(2)}, u32[]{:S(2)}) %all-to-all-start.2) | async-done | bytes 8388640 | tf_op jit(solution)/shard_map/all_to_all | solution.py:18
  259.1 0.0 copy-start
  259.1 8.6 %copy.15 = bf16[2,16,64,2048]{3,2,1,0:T(8,128)(2,1)} copy(bf16[2,16,64,2048]{3,2,0,1:T(8,128)(2,1)} %bitcast.6) | data formatting | bytes 16777216 | tf_op jit(solution)/shard_map/transpose | solution.py:21
  267.7 0.0 all-gather.3.cloned.1.call-done
  267.7 0.0 copy-done
  267.7 16.0 %convolution_convert_fusion = bf16[512,2048]{1,0:T(8,128)(2,1)} fusion(bf16[2048,2048]{1,0:T(8,128)(2,1)} %bitcast.20, bf16[2048,2048]{1,0:T(8,128)(2,1)} %all-gather.3.cloned.1.call-done, bf16[512,2048]{1,0:T(8,128)(2,1)S(1)} %copy-done, f32[512]{0:T(512)S(1)} %add_rsqrt_fusion), kind=kOutput, calls=%fused_computation.5 | convolution fusion | flops 8597274624 | bytes 20973568 | tf_op jit(solution)/shard_map/dot_general | solution.py:29
  283.7 0.0 reduce-scatter.2.cloned.1.call-update
  283.8 12.2 %copy.16 = bf16[2048,2048]{1,0:T(8,128)(2,1)} copy(bf16[2048,2048]{0,1:T(8,128)(2,1)} %bitcast.21) | data formatting | bytes 16777216
  296.0 50.7 %reduce-scatter.2.cloned.1.call-done = bf16[512,1024]{1,0:T(8,128)(2,1)} async-done(((bf16[512,2048]{1,0:T(8,128)(2,1)}), bf16[512,1024]{1,0:T(8,128)(2,1)}) %reduce-scatter.2.cloned.1.call-update) | async-done | bytes 1048592 | tf_op jit(solution)/shard_map/reduce_scatter | solution.py:30
  346.7 8.4 %copy.18 = bf16[2048,2048]{1,0:T(8,128)(2,1)} copy(bf16[2048,2048]{1,0:T(8,128)(2,1)} %all-gather.3.cloned.1.call-done) | data formatting | bytes 16777216
  (1 shorter events, 0.0 us)
Async XLA Ops:
  7.2 52.0 %all-gather.5.cloned.1.call-start = ((), (), s32[]{:S(2)}) async-start(), calls=%async_computation.5 | async-start | bytes 3145728 | tf_op jit(solution)/shard_map/all_gather | solution.py:23
  53.1 5.0 %copy-start.1 = (f32[128,2048]{1,0:T(8,128)S(1)}, f32[128,2048]{1,0:T(8,128)}, u32[]{:S(2)}) copy-start(f32[128,2048]{1,0:T(8,128)} %param.6) | copy-start | bytes 3145732
  53.2 5.0 %copy-start.2 = (f32[128]{0:T(128)S(1)}, f32[128]{0:T(128)}, u32[]{:S(2)}) copy-start(f32[128]{0:T(128)} %param.5) | copy-start | bytes 1540
  53.2 206.0 %all-to-all-start.2 = ((bf16[16,128,2048]{2,1,0:T(8,128)(2,1)}), bf16[16,128,2048]{2,1,0:T(8,128)(2,1)}, u32[]{:S(2)}, u32[]{:S(2)}) async-start(bf16[16,128,2048]{2,1,0:T(8,128)(2,1)} %stack.5), calls=%async_computation.2 | async-start | bytes 16777216 | tf_op jit(solution)/shard_map/all_to_all | solution.py:18
  58.1 209.7 %all-gather.3.cloned.1.call-start = ((), (), s32[]{:S(2)}) async-start(), calls=%async_computation.4 | async-start | bytes 8912896 | tf_op jit(solution)/shard_map/all_gather | solution.py:10
  59.1 287.6 %reduce-scatter.2.cloned.1.call-start = ((), (), s32[]{:S(2)}) async-start(), calls=%async_computation.6 | async-start | bytes 3145728 | tf_op jit(solution)/shard_map/reduce_scatter | solution.py:30
  259.1 8.6 %copy-start = (bf16[512,2048]{1,0:T(8,128)(2,1)S(1)}, bf16[512,2048]{1,0:T(8,128)(2,1)}, u32[]{:S(2)}) copy-start(bf16[512,2048]{1,0:T(8,128)(2,1)} %all-gather.5.cloned.1.call-done) | copy-start | bytes 6291460
Sparse Core Ops, SparseCore 0:
  9.5 41.4 all-gather.4
  61.6 183.0 all-gather.2
  283.9 62.7 reduce-scatter.1
